TPU v7x, 32 devices: a whole 2x2x4 slice. The times are simulated.
32 devices in a mesh: sp: 8 (over z, core), tp: 4 (over y, x).
Axes of the slice: x: 2, y: 2, z: 4, core: 2. Of those that a mesh axis runs over, the one named last changes fastest.
Arguments:
- query_a: bfloat16 [1024, 1024], P('tp', 'sp'), may hold values from -16 to 16
- key_a: bfloat16 [1024, 1024], P('tp', 'sp'), may hold values from -6 to 6
- value_a: bfloat16 [1024, 1024], P('tp', 'sp'), may hold values from -6 to 6
- cumlog_a: float32 [16, 1024], P('tp'), as said below
- query_b: bfloat16 [2048, 1024], P('tp', 'sp'), may hold values from -16 to 16
- key_b: bfloat16 [2048, 1024], P('tp', 'sp'), may hold values from -6 to 6
- value_b: bfloat16 [2048, 1024], P('tp', 'sp'), may hold values from -6 to 6
- cumlog_b: float32 [16, 1024], P('tp'), as said below
- out_weight_a: bfloat16 [1024, 2048], P('tp'), may hold values from -0.375 to 0.375
- out_weight_b: bfloat16 [2048, 2048], P('tp'), may hold values from -0.25 to 0.25
- residual: bfloat16 [1024, 2048], P(('sp', 'tp')), may hold values from -6 to 6
- norm_gain: float32 [2048], replicated, may hold values from 0.1 to 1.9
- expert_ids: int32 [1024, 2], P('sp'), may hold values from 0 to 7, as said below
- route_weight: float32 [1024, 2], P('sp'), may hold values from 0.1 to 1
- gate_w: bfloat16 [8, 2048, 1024], P('sp', None, 'tp'), may hold values from -0.125 to 0.125
- up_w: bfloat16 [8, 2048, 1024], P('sp', None, 'tp'), may hold values from -0.125 to 0.125
- down_w: bfloat16 [8, 1024, 2048], P('sp', None, 'tp'), may hold values from -0.1875 to 0.1875
Outputs:
- layer_out: bfloat16 [1024, 2048], P('sp', 'tp')
Inputs may be any that keep to these rules, and one draw needn't show every extreme that they name: `expert_ids`: each row names two different experts of one group (expert e is in group e // 2). In every aligned block of 128 rows (one index of sp) no expert is named more than 64 times, and every expert of one group, the same group for all blocks, is named exactly 64 times. `cumlog_a`: along positions the values of each head never increase. `cumlog_b`: along positions the values of each head never increase.
All inputs are finite; a program needn't handle non-finite values.
Results may differ from a plain program's by a relative error of at most 0.017.
Values may be sent and summed in bfloat16 or wider, within the bound.
A program may use at most 64 MiB of HBM per device.

v0:
```python
import jax
import jax.numpy as jnp
from jax import lax
from jax.sharding import PartitionSpec as P

HDA = 64
HDB = 128
GROUPS = 4
TOP = 2
norm_eps = 1e-05


def fold_group(state, queries, keys_piece, values_piece, cum_query, cum_key, visible, head_size):
    best, total, accum = state
    heads = best.shape[0]
    count = keys_piece.shape[1]
    key_grid = keys_piece.reshape(heads, head_size, count)
    value_grid = values_piece.reshape(heads, head_size, count)
    scores = jnp.einsum(
        "hdq,hdk->hqk", queries, key_grid, preferred_element_type=jnp.float32
    ) * head_size ** (-0.5)
    scores = scores + cum_query[:, :, None] - cum_key[:, None, :]
    scores = jnp.where(visible, scores, -jnp.inf)
    best_new = jnp.max(scores, axis=-1)
    shift = jnp.where(best_new > -jnp.inf, best_new, 0.0)
    keep_old = jnp.exp(best - shift)
    weights = jnp.exp(scores - shift[:, :, None])
    total_new = total * keep_old + jnp.sum(weights, axis=-1)
    added = jnp.einsum(
        "hqk,hdk->hdq", weights.astype(jnp.bfloat16), value_grid, preferred_element_type=jnp.float32
    )
    return (best_new, total_new, accum * keep_old[:, None, :] + added)


def empty_state(heads, head_size, length):
    return (
        jnp.full((heads, length), -jnp.inf, jnp.float32),
        jnp.zeros((heads, length), jnp.float32),
        jnp.zeros((heads, head_size, length), jnp.float32),
    )


def finish_state(state):
    accum = state[2] / state[1][:, None, :]
    return accum.astype(jnp.bfloat16).reshape(-1, accum.shape[2])


def per_device(
    query_a,
    key_a,
    value_a,
    cumlog_a,
    query_b,
    key_b,
    value_b,
    cumlog_b,
    out_weight_a,
    out_weight_b,
    residual,
    norm_gain,
    expert_ids,
    route_weight,
    gate_w,
    up_w,
    down_w,
):
    local_tokens = query_a.shape[1]
    heads_a = cumlog_a.shape[0]
    heads_b = cumlog_b.shape[0]
    my_start = lax.axis_index("sp") * local_tokens
    last_query = my_start + local_tokens - 1
    query_pos = my_start + jnp.arange(local_tokens, dtype=jnp.int32)
    cum_query_a = lax.dynamic_slice_in_dim(cumlog_a, my_start, local_tokens, 1)
    cum_query_b = lax.dynamic_slice_in_dim(cumlog_b, my_start, local_tokens, 1)
    grid_a = query_a.reshape(heads_a, HDA, local_tokens)
    grid_b = query_b.reshape(heads_b, HDB, local_tokens)
    keys_a = lax.all_gather(key_a, "sp", axis=1, tiled=True)
    vals_a = lax.all_gather(value_a, "sp", axis=1, tiled=True)
    keys_b = lax.all_gather(key_b, "sp", axis=1, tiled=True)
    vals_b = lax.all_gather(value_b, "sp", axis=1, tiled=True)
    count = keys_a.shape[1]

    def visit(state):
        key_pos = jnp.arange(count, dtype=jnp.int32)
        visible = key_pos[None, None, :] <= query_pos[None, :, None]
        new_a = fold_group(state[0], grid_a, keys_a, vals_a, cum_query_a, cumlog_a, visible, HDA)
        new_b = fold_group(state[1], grid_b, keys_b, vals_b, cum_query_b, cumlog_b, visible, HDB)
        return (new_a, new_b)

    def leave(state):
        return state

    state_a, state_b = lax.cond(
        jnp.int32(0) <= last_query,
        visit,
        leave,
        (empty_state(heads_a, HDA, local_tokens), empty_state(heads_b, HDB, local_tokens)),
    )
    attn_a = finish_state(state_a)
    attn_b = finish_state(state_b)
    term = lax.dot_general(
        attn_a, out_weight_a, (((0,), (0,)), ((), ())), preferred_element_type=jnp.float32
    )
    mixed = lax.psum_scatter(
        (
            term
            + lax.dot_general(
                attn_b, out_weight_b, (((0,), (0,)), ((), ())), preferred_element_type=jnp.float32
            )
        ).astype(jnp.bfloat16),
        "tp",
        scatter_dimension=0,
        tiled=True,
    ).astype(jnp.float32)
    summed = residual.astype(jnp.float32) + mixed
    center = summed - jnp.mean(summed, axis=-1, keepdims=True)
    variance = jnp.mean(center * center, axis=-1, keepdims=True)
    normed = (center * lax.rsqrt(variance + norm_eps) * norm_gain).astype(jnp.bfloat16)
    normed_all = lax.all_gather(normed, "tp", axis=0, tiled=True)
    experts = lax.axis_size("sp")
    group_size = experts // GROUPS
    capacity = local_tokens // group_size
    features = normed_all.shape[1]
    flat_ids = expert_ids.reshape(-1)
    marks = (flat_ids[:, None] == jnp.arange(experts, dtype=jnp.int32)[None, :]).astype(jnp.int32)
    rank = jnp.sum((jnp.cumsum(marks, axis=0) - marks) * marks, axis=1)
    slot = flat_ids * capacity + rank
    token_of = jnp.arange(local_tokens * TOP, dtype=jnp.int32) // TOP
    table = jnp.zeros((experts * capacity,), jnp.int32).at[slot].set(token_of)
    filled = jnp.zeros((experts * capacity,), jnp.bfloat16).at[slot].set(1.0)
    send = (normed_all[table] * filled[:, None]).reshape(experts, capacity, features)
    rows = lax.all_to_all(send, "sp", split_axis=0, concat_axis=0, tiled=True)
    sources, items, row_width = rows.shape
    flat_rows = rows.reshape(sources * items, row_width)
    gate = jnp.dot(flat_rows, gate_w[0], preferred_element_type=jnp.float32)
    upper = jnp.dot(flat_rows, up_w[0], preferred_element_type=jnp.float32)
    hidden = (jax.nn.silu(gate) * upper).astype(jnp.bfloat16).reshape(sources, items, -1)
    hidden_all = lax.all_gather(hidden, "tp", axis=2, tiled=True)
    result = jnp.dot(
        hidden_all.reshape(sources * items, -1), down_w[0], preferred_element_type=jnp.float32
    )
    result = result.astype(jnp.bfloat16).reshape(sources, items, -1)
    returned = lax.all_to_all(result, "sp", split_axis=0, concat_axis=0, tiled=True)
    flat_back = returned.reshape(experts * capacity, -1)
    picked = flat_back[slot].reshape(local_tokens, TOP, -1).astype(jnp.float32)
    routed = jnp.sum(picked * route_weight[:, :, None], axis=1)
    columns = routed.shape[1]
    own_cols = lax.dynamic_slice_in_dim(normed_all, lax.axis_index("tp") * columns, columns, 1)
    return (own_cols.astype(jnp.float32) + routed).astype(jnp.bfloat16)


def solution(mesh):
    placed = (
        P("tp", "sp"),
        P("tp", "sp"),
        P("tp", "sp"),
        P("tp", None),
        P("tp", "sp"),
        P("tp", "sp"),
        P("tp", "sp"),
        P("tp", None),
        P("tp", None),
        P("tp", None),
        P(("sp", "tp"), None),
        P(),
        P("sp", None),
        P("sp", None),
        P("sp", None, "tp"),
        P("sp", None, "tp"),
        P("sp", None, "tp"),
    )
    return jax.shard_map(
        per_device, mesh=mesh, in_specs=placed, out_specs=P("sp", "tp"), check_vma=False
    )
```

profile of v0, /device:TPU:0, one launch (start us, length us, event | category | flops | bytes accessed | tf_op | source)
XLA Modules:
  0.0 229.1 jit_solution(7319173430591822474)
XLA Ops:
  6.5 0.7 all-gather.4.cloned.1.call-update
  7.3 0.7 all-gather.6.cloned.1.call-update
  8.1 0.8 copy.27
  8.8 0.1 eq.29
  9.0 0.7 eq.25
  9.7 0.7 broadcast_multiply_fusion.1
  10.4 0.1 copy.26
  10.5 0.1 mul.103
  10.6 17.6 %all_gather.18 = bf16[256,1024]{1,0:T(8,128)(2,1)S(1)} all-gather(bf16[256,128]{1,0:T(8,128)(2,1)} %param.20), channel_id=1, replica_groups=mesh['sp'=8,'tp'=4] {'sp'}, dimensions={1}, use_global_device_ids=true | all-gather | bytes 589824 | tf_op jit(solution)/shard_map/all_gather | solution.py:77
  28.2 14.7 %all_gather.19 = bf16[256,1024]{1,0:T(8,128)(2,1)S(1)} all-gather(bf16[256,128]{1,0:T(8,128)(2,1)} %param.21), channel_id=1, replica_groups=mesh['sp'=8,'tp'=4] {'sp'}, dimensions={1}, use_global_device_ids=true | all-gather | bytes 589824 | tf_op jit(solution)/shard_map/all_gather | solution.py:78
  42.9 19.9 %all-gather.6.cloned.1.call-done = bf16[512,1024]{1,0:T(8,128)(2,1)} async-done(((bf16[512,128]{1,0:T(8,128)(2,1)}), bf16[512,1024]{1,0:T(8,128)(2,1)}) %all-gather.6.cloned.1.call-update) | async-done | bytes 1048592 | tf_op jit(solution)/shard_map/all_gather | solution.py:80
  62.8 7.6 %conditional.1 = (f32[4,128]{1,0:T(4,128)S(1)}, f32[4,64,128]{2,1,0:T(8,128)S(1)}, f32[4,128]{1,0:T(4,128)S(1)}, f32[4,128,128]{2,1,0:T(8,128)S(1)}) conditional(s32[]{:T(128)} %convert_element_type.59, () %tuple.20, (s32[]{:T(128)}, s32[128]{0:T(128)S(1)}, bf16[256,128]{1,0:T(8,128)(2,1)}, bf16[256,1024]{1,0:T(8,128)(2,1)S(1)}, f32[4,1024]{1,0:T(4,128)}, ...), branch_computations={%region_0.0_spmd, %region_1.6_spmd} | conditional | flops 412324992 | bytes 26306234 | solution.py:93
  62.8 0.8 constant_dynamic-slice_fusion
  63.6 0.1 iota_compare_fusion
  63.7 1.6 fusion.27
  65.4 0.5 fusion.1
  65.9 0.6 fusion.5
  66.6 0.8 fusion.28
  67.4 0.5 fusion.3
  68.0 1.3 fusion.4
  69.3 1.1 copy.32
  70.4 1.6 fusion.29
  72.1 1.3 fusion.12
  73.4 0.6 reduce-window.6
  74.0 0.2 slice_reduce_fusion
  74.3 0.1 fusion.21
  74.4 1.4 scatter_custom_fusion
  75.8 2.2 scatter_custom_fusion.1
  78.0 19.3 %reduce-scatter.2.cloned.1.call-done = bf16[32,2048]{1,0:T(8,128)(2,1)} async-done(((bf16[128,2048]{1,0:T(8,128)(2,1)}), bf16[32,2048]{1,0:T(8,128)(2,1)}) %reduce-scatter.2.cloned.1.call-update) | async-done | bytes 131088 | tf_op jit(solution)/shard_map/reduce_scatter | solution.py:104
  97.3 1.0 fusion.19
  98.4 1.1 multiply_reduce_fusion.1
  99.5 1.0 multiply_convert_fusion
  100.5 10.2 %all_gather.22 = bf16[128,2048]{1,0:T(8,128)(2,1)S(1)} all-gather(bf16[32,2048]{1,0:T(8,128)(2,1)S(1)} %multiply_convert_fusion), channel_id=1, replica_groups=mesh['sp'=8,'tp'=4] {'tp'}, dimensions={0}, use_global_device_ids=true | all-gather | bytes 655360 | tf_op jit(solution)/shard_map/all_gather | solution.py:119
  110.8 3.3 %gather_fusion = bf16[512,2048]{1,0:T(8,128)(2,1)} fusion(bf16[128,2048]{1,0:T(8,128)(2,1)S(1)} %all_gather.22, s32[1024]{0:T(1024)S(1)} %pad_clamp_fusion.1), kind=kCustom, calls=%fused_computation | custom fusion | bytes 4196352 | tf_op jit(solution)/shard_map/gather | solution.py:131
  114.1 1.8 broadcast_multiply_fusion
  115.9 53.6 %all_to_all.10 = bf16[8,64,2048]{2,1,0:T(8,128)(2,1)S(1)} all-to-all(bf16[8,64,2048]{2,1,0:T(8,128)(2,1)S(1)} %broadcast_multiply_fusion), channel_id=1, replica_groups=mesh['sp'=8,'tp'=4] {'sp'}, dimensions={0} | all-to-all | bytes 4194304 | tf_op jit(solution)/shard_map/all_to_all | solution.py:132
  169.5 0.7 fusion.16
  170.3 0.5 copy-done.8
  170.8 1.4 fusion.13
  172.2 24.5 %all-gather.8.cloned.1.call-done = bf16[8,64,1024]{2,1,0:T(8,128)(2,1)} async-done(((bf16[8,64,256]{2,1,0:T(8,128)(2,1)}), bf16[8,64,1024]{2,1,0:T(8,128)(2,1)}) %all-gather.8.cloned.1.call-update) | async-done | bytes 1048592 | tf_op jit(solution)/shard_map/all_gather | solution.py:138
  196.7 3.1 %convolution_convert_fusion = bf16[512,512]{1,0:T(8,128)(2,1)} fusion(bf16[512,1024]{1,0:T(8,128)(2,1)} %bitcast.66, bf16[1,1024,512]{2,1,0:T(8,128)(2,1)} %param.35), kind=kOutput, calls=%fused_computation.30 | convolution fusion | flops 537133056 | bytes 2621440 | tf_op jit(solution)/shard_map/dot_general | solution.py:139
  199.8 4.6 %all-to-all-start.1 = ((bf16[8,64,512]{2,1,0:T(8,128)(2,1)}), bf16[8,64,512]{2,1,0:T(8,128)(2,1)S(1)}, u32[]{:S(2)}, u32[]{:S(2)}) async-start(bf16[8,64,512]{2,1,0:T(8,128)(2,1)} %bitcast.57), calls=%async_computation.2 | async-start | bytes 1048576 | tf_op jit(solution)/shard_map/all_to_all | solution.py:143
  204.4 0.1 copy.29
  204.5 15.2 %all-to-all-done.1 = bf16[8,64,512]{2,1,0:T(8,128)(2,1)S(1)} async-done(((bf16[8,64,512]{2,1,0:T(8,128)(2,1)}), bf16[8,64,512]{2,1,0:T(8,128)(2,1)S(1)}, u32[]{:S(2)}, u32[]{:S(2)}) %all-to-all-start.1) | async-done | bytes 524320 | tf_op jit(solution)/shard_map/all_to_all | solution.py:143
  219.7 1.2 gather_fusion.1
  220.9 0.3 reshape.190
  221.2 0.7 multiply_reduce_fusion
  221.9 0.7 add_convert_fusion
  (48 shorter events, 0.5 us)
Async XLA Ops:
  6.5 65.5 %copy-start = (bf16[512,2048]{1,0:T(8,128)(2,1)S(1)}, bf16[512,2048]{1,0:T(8,128)(2,1)}, u32[]{:S(2)}) copy-start(bf16[512,2048]{1,0:T(8,128)(2,1)} %param.28) | copy-start | bytes 6291460
  6.5 36.4 %all-gather.4.cloned.1.call-start = ((), (), s32[]{:S(2)}) async-start(), calls=%async_computation.3 | async-start | bytes 1179648 | tf_op jit(solution)/shard_map/all_gather | solution.py:79
  7.3 55.5 %all-gather.6.cloned.1.call-start = ((), (), s32[]{:S(2)}) async-start(), calls=%async_computation.4 | async-start | bytes 1179648 | tf_op jit(solution)/shard_map/all_gather | solution.py:80
  8.0 89.3 %reduce-scatter.2.cloned.1.call-start = ((), (), s32[]{:S(2)}) async-start(), calls=%async_computation.5 | async-start | bytes 655360 | tf_op jit(solution)/shard_map/reduce_scatter | solution.py:104
  65.4 1.2 copy-start.6
  65.4 1.2 copy-start.9
  65.4 1.2 copy-start.10
  66.6 1.4 copy-start.2
  72.0 2.2 copy-start.4
  72.0 25.3 %copy-start.1 = (bf16[32,2048]{1,0:T(8,128)(2,1)S(1)}, bf16[32,2048]{1,0:T(8,128)(2,1)}, u32[]{:S(2)}) copy-start(bf16[32,2048]{1,0:T(8,128)(2,1)} %param.29) | copy-start | bytes 393220
  72.0 27.5 %copy-start.3 = (f32[2048]{0:T(1024)S(1)}, f32[2048]{0:T(1024)}, u32[]{:S(2)}) copy-start(f32[2048]{0:T(1024)} %param.30) | copy-start | bytes 24580
  73.3 123.4 %all-gather.8.cloned.1.call-start = ((), (), s32[]{:S(2)}) async-start(), calls=%async_computation.6 | async-start | bytes 1310720 | tf_op jit(solution)/shard_map/all_gather | solution.py:138
  115.9 53.6 %copy-start.7 = (bf16[1,2048,256]{2,1,0:T(8,128)(2,1)S(1)}, bf16[1,2048,256]{2,1,0:T(8,128)(2,1)}, u32[]{:S(2)}) copy-start(bf16[1,2048,256]{2,1,0:T(8,128)(2,1)} %param.33) | copy-start | bytes 3145732
  169.5 1.2 copy-start.8
  196.7 7.7 %copy-start.5 = (f32[128,2]{0,1:T(2,128)S(1)}, f32[128,2]{0,1:T(2,128)}, u32[]{:S(2)}) copy-start(f32[128,2]{0,1:T(2,128)} %param.32) | copy-start | bytes 3076
  199.8 19.9 %all-to-all-start.1 = ((bf16[8,64,512]{2,1,0:T(8,128)(2,1)}), bf16[8,64,512]{2,1,0:T(8,128)(2,1)S(1)}, u32[]{:S(2)}, u32[]{:S(2)}) async-start(bf16[8,64,512]{2,1,0:T(8,128)(2,1)} %bitcast.57), calls=%async_computation.2 | async-start | bytes 1048576 | tf_op jit(solution)/shard_map/all_to_all | solution.py:143
Sparse Core Ops, SparseCore 0:
  8.9 27.7 all-gather.3
  38.3 24.4 all-gather.5
  73.5 23.8 reduce-scatter.1
  172.3 24.3 all-gather.7
where the time goes:
time: 230 us; the launch traced here: 229 us
  blocking collectives  96.1 us (42%)
  waiting for transfers between devices  80.3 us (35%)
  between operations  13.3 us (6%)
  local copies, waits for them, and re-layouts  13.2 us (6%)
  matrix products  12.4 us (5%)
  other arithmetic  9.06 us (4%)
  starting transfers between devices  4.73 us (2%)
    all_to_all x1, blocking collectives, per_device(): rows = lax.all_to_all(send, 'sp', split_axis=0, concat_axis=0, tiled=True)  53.6 us
    all_gather x1, waiting for transfers between devices, per_device(): hidden_all = lax.all_gather(hidden, 'tp', axis=2, tiled=True)  24.5 us
    all_gather x1, waiting for transfers between devices, per_device(): vals_b = lax.all_gather(value_b, 'sp', axis=1, tiled=True)  19.9 us
    reduce_scatter x1, waiting for transfers between devices, per_device(): lax.psum_scatter((term + lax.dot_general(attn_b, out_weight_b, (((0,), (0...  19.3 us
    all_gather x1, blocking collectives, per_device(): keys_a = lax.all_gather(key_a, 'sp', axis=1, tiled=True)  17.6 us
    all_to_all x1, waiting for transfers between devices, per_device(): lax.all_to_all(result, 'sp', split_axis=0, concat_axis=0, tiled=True)  15.2 us
    all_gather x1, blocking collectives, per_device(): vals_a = lax.all_gather(value_a, 'sp', axis=1, tiled=True)  14.7 us
    all_gather x1, blocking collectives, per_device(): normed_all = lax.all_gather(normed, 'tp', axis=0, tiled=True)  10.2 us
  transfers between devices with their start and end apart: 5, of which 4 were waited for; matrix products, arithmetic and copies ran while one was open for 3% of the time, Pallas kernels for 0%

commit v1 on v0

--- a/solution.py
+++ b/solution.py
@@ -75,7 +75,14 @@
     grid_a = query_a.reshape(heads_a, HDA, local_tokens)
     grid_b = query_b.reshape(heads_b, HDB, local_tokens)
     keys_a = lax.all_gather(key_a, "sp", axis=1, tiled=True)
-    vals_a = lax.all_gather(value_a, "sp", axis=1, tiled=True)
+    peers = lax.axis_size("sp")
+    right = [(i, (i + 1) % peers) for i in range(peers)]
+    terms = [value_a]
+    for far in range(1, peers):
+        terms = [lax.ppermute(terms[0], "sp", right), *terms]
+    whole = jnp.concatenate(terms, axis=1)
+    turn = (lax.axis_index("sp") + 1) * terms[-1].shape[1]
+    vals_a = jnp.roll(whole, turn, axis=1)
     keys_b = lax.all_gather(key_b, "sp", axis=1, tiled=True)
     vals_b = lax.all_gather(value_b, "sp", axis=1, tiled=True)
     count = keys_a.shape[1]

time: 230 us -> 237 us (1.030)
  blocking collectives: 96.1 us -> 80.4 us
  waiting for transfers between devices: 80.3 us -> 92.7 us
  local copies, waits for them, and re-layouts: 13.2 us -> 20.5 us
    ppermute x0 -> x7, waiting for transfers between devices: none -> 33.6 us  [per_device(): terms = [lax.ppermute(terms[0], 'sp', right), *terms]]
    all_gather x1, waiting for transfers between devices: 19.9 us -> 0.02 us  [per_device(): vals_b = lax.all_gather(value_b, 'sp', axis=1, tiled=True)]
    all_gather x1 -> x0, blocking collectives: 14.7 us -> none  [per_device(): vals_a = lax.all_gather(value_a, 'sp', axis=1, tiled=True)]
    unnamed x16 -> x39, local copies, waits for them, and re-layouts: 1.44 us -> 5.41 us
  transfers between devices with their start and end apart: 5 -> 12, of which waited for: 4 -> 9; matrix products, arithmetic and copies ran while one was open for 3% -> 5% of each run, Pallas kernels for 0% -> 0%
where the time goes in v1:
time: 237 us; the launch traced here: 236 us
  waiting for transfers between devices  92.7 us (39%)
  blocking collectives  80.4 us (34%)
  local copies, waits for them, and re-layouts  20.5 us (9%)
  matrix products  13.8 us (6%)
  between operations  13.4 us (6%)
  other arithmetic  9.71 us (4%)
  starting transfers between devices  5.67 us (2%)
    all_to_all x1, blocking collectives, per_device(): rows = lax.all_to_all(send, 'sp', split_axis=0, concat_axis=0, tiled=True)  53.6 us
    ppermute x7, waiting for transfers between devices, per_device(): terms = [lax.ppermute(terms[0], 'sp', right), *terms]  33.6 us
    all_gather x1, waiting for transfers between devices, per_device(): hidden_all = lax.all_gather(hidden, 'tp', axis=2, tiled=True)  24.5 us
    reduce_scatter x1, waiting for transfers between devices, per_device(): lax.psum_scatter((term + lax.dot_general(attn_b, out_weight_b, (((0,), (0...  18.7 us
    all_gather x1, blocking collectives, per_device(): keys_a = lax.all_gather(key_a, 'sp', axis=1, tiled=True)  16.5 us
    all_to_all x1, waiting for transfers between devices, per_device(): lax.all_to_all(result, 'sp', split_axis=0, concat_axis=0, tiled=True)  15.2 us
    all_gather x1, blocking collectives, per_device(): normed_all = lax.all_gather(normed, 'tp', axis=0, tiled=True)  10.3 us
    unnamed x39, local copies, waits for them, and re-layouts  5.41 us
  transfers between devices with their start and end apart: 12, of which 9 were waited for; matrix products, arithmetic and copies ran while one was open for 5% of the time, Pallas kernels for 0%

profile of v1, /device:TPU:0, one launch (start us, length us, event | category | flops | bytes accessed | tf_op | source)
XLA Modules:
  0.0 236.3 jit_solution(11625262327277251841)
XLA Ops:
  6.5 0.7 all-gather.4.cloned.1.call-update
  7.3 0.5 collective-permute-start
  7.9 6.2 %collective-permute-done = bf16[256,128]{1,0:T(8,128)(2,1)S(1)} collective-permute-done((bf16[256,128]{1,0:T(8,128)(2,1)}, bf16[256,128]{1,0:T(8,128)(2,1)S(1)}, u32[]{:S(2)}, u32[]{:S(2)}) %collective-permute-start) | collective-permute-done | bytes 65568 | tf_op jit(solution)/shard_map/ppermute | solution.py:82
  14.0 5.5 %collective-permute-done.1 = bf16[256,128]{1,0:T(8,128)(2,1)S(1)} collective-permute-done((bf16[256,128]{1,0:T(8,128)(2,1)S(1)}, bf16[256,128]{1,0:T(8,128)(2,1)S(1)}, u32[]{:S(2)}, u32[]{:S(2)}) %collective-permute-start.1) | collective-permute-done | bytes 65568 | tf_op jit(solution)/shard_map/ppermute | solution.py:82
  19.5 6.7 %collective-permute-done.2 = bf16[256,128]{1,0:T(8,128)(2,1)S(1)} collective-permute-done((bf16[256,128]{1,0:T(8,128)(2,1)S(1)}, bf16[256,128]{1,0:T(8,128)(2,1)S(1)}, u32[]{:S(2)}, u32[]{:S(2)}) %collective-permute-start.2) | collective-permute-done | bytes 65568 | tf_op jit(solution)/shard_map/ppermute | solution.py:82
  26.3 6.6 %collective-permute-done.3 = bf16[256,128]{1,0:T(8,128)(2,1)S(1)} collective-permute-done((bf16[256,128]{1,0:T(8,128)(2,1)S(1)}, bf16[256,128]{1,0:T(8,128)(2,1)S(1)}, u32[]{:S(2)}, u32[]{:S(2)}) %collective-permute-start.3) | collective-permute-done | bytes 65568 | tf_op jit(solution)/shard_map/ppermute | solution.py:82
  33.0 5.4 %collective-permute-done.4 = bf16[256,128]{1,0:T(8,128)(2,1)S(1)} collective-permute-done((bf16[256,128]{1,0:T(8,128)(2,1)S(1)}, bf16[256,128]{1,0:T(8,128)(2,1)S(1)}, u32[]{:S(2)}, u32[]{:S(2)}) %collective-permute-start.4) | collective-permute-done | bytes 65568 | tf_op jit(solution)/shard_map/ppermute | solution.py:82
  38.4 16.5 %all_gather.15 = bf16[256,1024]{1,0:T(8,128)(2,1)} all-gather(bf16[256,128]{1,0:T(8,128)(2,1)} %param.20), channel_id=1, replica_groups=mesh['sp'=8,'tp'=4] {'sp'}, dimensions={1}, use_global_device_ids=true | all-gather | bytes 589824 | tf_op jit(solution)/shard_map/all_gather | solution.py:77
  55.3 0.7 broadcast_multiply_fusion.1
  56.0 0.8 copy.31
  56.9 0.7 eq.28
  57.9 3.1 %collective-permute-done.6 = bf16[256,128]{1,0:T(8,128)(2,1)} collective-permute-done((bf16[256,128]{1,0:T(8,128)(2,1)S(1)}, bf16[256,128]{1,0:T(8,128)(2,1)}, u32[]{:S(2)}, u32[]{:S(2)}) %collective-permute-start.6) | collective-permute-done | bytes 65568 | tf_op jit(solution)/shard_map/ppermute | solution.py:82
  61.0 0.9 constant_dynamic-update-slice_fusion.15
  61.9 0.9 constant_dynamic-update-slice_fusion.14
  62.9 0.9 constant_dynamic-update-slice_fusion.7
  63.8 0.9 constant_dynamic-update-slice_fusion.6
  64.8 0.6 iota.27
  65.8 13.7 %conditional.1 = (f32[4,128]{1,0:T(4,128)S(1)}, f32[4,64,128]{2,1,0:T(8,128)S(1)}, f32[4,128]{1,0:T(4,128)S(1)}, f32[4,128,128]{2,1,0:T(8,128)S(1)}) conditional(s32[]{:T(128)} %convert_element_type.61, () %tuple.26, (s32[]{:T(128)}, s32[128]{0:T(128)}, bf16[256,128]{1,0:T(8,128)(2,1)}, bf16[256,1024]{1,0:T(8,128)(2,1)}, f32[4,1024]{1,0:T(4,128)}, ...), branch_computations={%region_0.1_spmd, %region_1.6_spmd.clone} | conditional | flops 412324992 | bytes 35219288 | solution.py:100
  65.8 0.9 constant_dynamic-slice_fusion
  66.6 0.7 broadcast_add_fusion
  67.4 1.8 fusion.26
  69.3 1.3 copy-done.1
  71.2 1.4 constant_dynamic-slice_fusion.1
  72.5 2.2 convolution_add_fusion.1
  74.7 1.8 fusion.27
  77.1 1.3 fusion.4
  78.4 1.1 copy.36
  79.9 1.3 fusion.11
  81.3 0.6 reduce-window.6
  82.2 1.4 scatter_custom_fusion
  83.6 2.2 scatter_custom_fusion.1
  85.9 18.7 %reduce-scatter.2.cloned.1.call-done = bf16[32,2048]{1,0:T(8,128)(2,1)} async-done(((bf16[128,2048]{1,0:T(8,128)(2,1)}), bf16[32,2048]{1,0:T(8,128)(2,1)}) %reduce-scatter.2.cloned.1.call-update) | async-done | bytes 131088 | tf_op jit(solution)/shard_map/reduce_scatter | solution.py:111
  104.6 1.0 fusion.18
  105.6 1.1 multiply_reduce_fusion.1
  106.7 1.0 multiply_convert_fusion
  107.8 10.3 %all_gather.18 = bf16[128,2048]{1,0:T(8,128)(2,1)S(1)} all-gather(bf16[32,2048]{1,0:T(8,128)(2,1)S(1)} %multiply_convert_fusion), channel_id=1, replica_groups=mesh['sp'=8,'tp'=4] {'tp'}, dimensions={0}, use_global_device_ids=true | all-gather | bytes 655360 | tf_op jit(solution)/shard_map/all_gather | solution.py:126
  118.0 3.3 %gather_fusion = bf16[512,2048]{1,0:T(8,128)(2,1)} fusion(bf16[128,2048]{1,0:T(8,128)(2,1)S(1)} %all_gather.18, s32[1024]{0:T(1024)S(1)} %pad_clamp_fusion.1), kind=kCustom, calls=%fused_computation | custom fusion | bytes 4196352 | tf_op jit(solution)/shard_map/gather | solution.py:138
  121.4 1.8 broadcast_multiply_fusion
  123.2 53.6 %all_to_all.10 = bf16[8,64,2048]{2,1,0:T(8,128)(2,1)S(1)} all-to-all(bf16[8,64,2048]{2,1,0:T(8,128)(2,1)S(1)} %broadcast_multiply_fusion), channel_id=1, replica_groups=mesh['sp'=8,'tp'=4] {'sp'}, dimensions={0} | all-to-all | bytes 4194304 | tf_op jit(solution)/shard_map/all_to_all | solution.py:139
  176.8 0.7 fusion.15
  178.0 1.4 fusion.12
  179.4 24.5 %all-gather.8.cloned.1.call-done = bf16[8,64,1024]{2,1,0:T(8,128)(2,1)} async-done(((bf16[8,64,256]{2,1,0:T(8,128)(2,1)}), bf16[8,64,1024]{2,1,0:T(8,128)(2,1)}) %all-gather.8.cloned.1.call-update) | async-done | bytes 1048592 | tf_op jit(solution)/shard_map/all_gather | solution.py:145
  203.9 3.1 %convolution_convert_fusion = bf16[512,512]{1,0:T(8,128)(2,1)} fusion(bf16[512,1024]{1,0:T(8,128)(2,1)} %bitcast.64, bf16[1,1024,512]{2,1,0:T(8,128)(2,1)} %param.35), kind=kOutput, calls=%fused_computation.30 | convolution fusion | flops 537133056 | bytes 2621440 | tf_op jit(solution)/shard_map/dot_general | solution.py:146
  207.0 4.6 %all-to-all-start.1 = ((bf16[8,64,512]{2,1,0:T(8,128)(2,1)}), bf16[8,64,512]{2,1,0:T(8,128)(2,1)S(1)}, u32[]{:S(2)}, u32[]{:S(2)}) async-start(bf16[8,64,512]{2,1,0:T(8,128)(2,1)} %bitcast.55), calls=%async_computation.2 | async-start | bytes 1048576 | tf_op jit(solution)/shard_map/all_to_all | solution.py:150
  211.7 15.2 %all-to-all-done.1 = bf16[8,64,512]{2,1,0:T(8,128)(2,1)S(1)} async-done(((bf16[8,64,512]{2,1,0:T(8,128)(2,1)}), bf16[8,64,512]{2,1,0:T(8,128)(2,1)S(1)}, u32[]{:S(2)}, u32[]{:S(2)}) %all-to-all-start.1) | async-done | bytes 524320 | tf_op jit(solution)/shard_map/all_to_all | solution.py:150
  226.9 1.2 gather_fusion.1
  228.4 0.7 multiply_reduce_fusion
  229.1 0.7 add_convert_fusion
  (86 shorter events, 4.7 us)
Async XLA Ops:
  6.5 73.3 %copy-start = (bf16[512,2048]{1,0:T(8,128)(2,1)S(1)}, bf16[512,2048]{1,0:T(8,128)(2,1)}, u32[]{:S(2)}) copy-start(bf16[512,2048]{1,0:T(8,128)(2,1)} %param.28) | copy-start | bytes 6291460
  6.5 56.3 %copy-start.6 = (bf16[256,128]{1,0:T(8,128)(2,1)S(1)}, bf16[256,128]{1,0:T(8,128)(2,1)}, u32[]{:S(2)}) copy-start(bf16[256,128]{1,0:T(8,128)(2,1)} %param.21) | copy-start | bytes 196612
  6.5 58.3 %all-gather.4.cloned.1.call-start = ((), (), s32[]{:S(2)}) async-start(), calls=%async_computation.3 | async-start | bytes 1179648 | tf_op jit(solution)/shard_map/all_gather | solution.py:86
  7.3 57.6 %all-gather.6.cloned.1.call-start = ((), (), s32[]{:S(2)}) async-start(), calls=%async_computation.4 | async-start | bytes 1179648 | tf_op jit(solution)/shard_map/all_gather | solution.py:87
  7.3 6.7 %collective-permute-start = (bf16[256,128]{1,0:T(8,128)(2,1)}, bf16[256,128]{1,0:T(8,128)(2,1)S(1)}, u32[]{:S(2)}, u32[]{:S(2)}) collective-permute-start(bf16[256,128]{1,0:T(8,128)(2,1)} %param.21), channel_id=1, source_target_pairs={{0,4},{4,8},{8,12},{12,16},{16,20},{20,24},{24,28},{28,0},{1,5},{5... | collective-permute-start | bytes 196616 | tf_op jit(solution)/shard_map/ppermute | solution.py:82
  14.0 5.5 %collective-permute-start.1 = (bf16[256,128]{1,0:T(8,128)(2,1)S(1)}, bf16[256,128]{1,0:T(8,128)(2,1)S(1)}, u32[]{:S(2)}, u32[]{:S(2)}) collective-permute-start(bf16[256,128]{1,0:T(8,128)(2,1)S(1)} %collective-permute-done), channel_id=1, source_target_pairs={{0,4},{4,8},{8,12},{12,16},{16,20},{20,24},{24,28},{28,0},{1,5},{5... | collective-permute-start | bytes 196616 | tf_op jit(solution)/shard_map/ppermute | solution.py:82
  19.5 6.7 %collective-permute-start.2 = (bf16[256,128]{1,0:T(8,128)(2,1)S(1)}, bf16[256,128]{1,0:T(8,128)(2,1)S(1)}, u32[]{:S(2)}, u32[]{:S(2)}) collective-permute-start(bf16[256,128]{1,0:T(8,128)(2,1)S(1)} %collective-permute-done.1), channel_id=1, source_target_pairs={{0,4},{4,8},{8,12},{12,16},{16,20},{20,24},{24,28},{28,0},{1,5},{5... | collective-permute-start | bytes 196616 | tf_op jit(solution)/shard_map/ppermute | solution.py:82
  26.3 6.6 %collective-permute-start.3 = (bf16[256,128]{1,0:T(8,128)(2,1)S(1)}, bf16[256,128]{1,0:T(8,128)(2,1)S(1)}, u32[]{:S(2)}, u32[]{:S(2)}) collective-permute-start(bf16[256,128]{1,0:T(8,128)(2,1)S(1)} %collective-permute-done.2), channel_id=1, source_target_pairs={{0,4},{4,8},{8,12},{12,16},{16,20},{20,24},{24,28},{28,0},{1,5},{5... | collective-permute-start | bytes 196616 | tf_op jit(solution)/shard_map/ppermute | solution.py:82
  32.9 5.5 %collective-permute-start.4 = (bf16[256,128]{1,0:T(8,128)(2,1)S(1)}, bf16[256,128]{1,0:T(8,128)(2,1)S(1)}, u32[]{:S(2)}, u32[]{:S(2)}) collective-permute-start(bf16[256,128]{1,0:T(8,128)(2,1)S(1)} %collective-permute-done.3), channel_id=1, source_target_pairs={{0,4},{4,8},{8,12},{12,16},{16,20},{20,24},{24,28},{28,0},{1,5},{5... | collective-permute-start | bytes 196616 | tf_op jit(solution)/shard_map/ppermute | solution.py:82
  32.9 71.6 %reduce-scatter.2.cloned.1.call-start = ((), (), s32[]{:S(2)}) async-start(), calls=%async_computation.5 | async-start | bytes 655360 | tf_op jit(solution)/shard_map/reduce_scatter | solution.py:111
  38.4 16.5 %collective-permute-start.5 = (bf16[256,128]{1,0:T(8,128)(2,1)S(1)}, bf16[256,128]{1,0:T(8,128)(2,1)S(1)}, u32[]{:S(2)}, u32[]{:S(2)}) collective-permute-start(bf16[256,128]{1,0:T(8,128)(2,1)S(1)} %collective-permute-done.4), channel_id=1, source_target_pairs={{0,4},{4,8},{8,12},{12,16},{16,20},{20,24},{24,28},{28,0},{1,5},{5... | collective-permute-start | bytes 196616 | tf_op jit(solution)/shard_map/ppermute | solution.py:82
  54.9 3.0 %copy-start.7 = (bf16[256,128]{1,0:T(8,128)(2,1)}, bf16[256,128]{1,0:T(8,128)(2,1)S(1)}, u32[]{:S(2)}) copy-start(bf16[256,128]{1,0:T(8,128)(2,1)S(1)} %collective-permute-done.5) | copy-start | bytes 196612
  54.9 6.1 %collective-permute-start.6 = (bf16[256,128]{1,0:T(8,128)(2,1)S(1)}, bf16[256,128]{1,0:T(8,128)(2,1)}, u32[]{:S(2)}, u32[]{:S(2)}) collective-permute-start(bf16[256,128]{1,0:T(8,128)(2,1)S(1)} %collective-permute-done.5), channel_id=1, source_target_pairs={{0,4},{4,8},{8,12},{12,16},{16,20},{20,24},{24,28},{28,0},{1,5},{5... | collective-permute-start | bytes 196616 | tf_op jit(solution)/shard_map/ppermute | solution.py:82
  64.8 1.0 copy-start.5
  65.8 13.7 %copy-start.3 = (bf16[256,2048]{1,0:T(8,128)(2,1)S(1)}, bf16[256,2048]{1,0:T(8,128)(2,1)}, u32[]{:S(2)}) copy-start(bf16[256,2048]{1,0:T(8,128)(2,1)} %param.27) | copy-start | bytes 3145732
  69.2 1.3 copy-start.1
  71.1 3.6 %copy-start.11 = (f32[4,1024]{1,0:T(4,128)S(1)}, f32[4,1024]{1,0:T(4,128)}, u32[]{:S(2)}) copy-start(f32[4,1024]{1,0:T(4,128)} %get-tuple-element.275) | copy-start | bytes 49156 | tf_op jit(solution)/shard_map/cond
  71.1 3.6 %copy-start.14 = (bf16[512,1024]{1,0:T(8,128)(2,1)S(1)}, bf16[512,1024]{1,0:T(8,128)(2,1)}, u32[]{:S(2)}) copy-start(bf16[512,1024]{1,0:T(8,128)(2,1)} %get-tuple-element.268) | copy-start | bytes 3145732 | tf_op jit(solution)/shard_map/cond
  74.7 2.4 copy-start.4
  79.9 2.2 copy-start.9
  79.9 24.7 %copy-start.2 = (bf16[32,2048]{1,0:T(8,128)(2,1)S(1)}, bf16[32,2048]{1,0:T(8,128)(2,1)}, u32[]{:S(2)}) copy-start(bf16[32,2048]{1,0:T(8,128)(2,1)} %param.29) | copy-start | bytes 393220
  79.9 26.8 %copy-start.8 = (f32[2048]{0:T(1024)S(1)}, f32[2048]{0:T(1024)}, u32[]{:S(2)}) copy-start(f32[2048]{0:T(1024)} %param.30) | copy-start | bytes 24580
  81.2 122.7 %all-gather.8.cloned.1.call-start = ((), (), s32[]{:S(2)}) async-start(), calls=%async_computation.6 | async-start | bytes 1310720 | tf_op jit(solution)/shard_map/all_gather | solution.py:145
  123.2 53.6 %copy-start.12 = (bf16[1,2048,256]{2,1,0:T(8,128)(2,1)S(1)}, bf16[1,2048,256]{2,1,0:T(8,128)(2,1)}, u32[]{:S(2)}) copy-start(bf16[1,2048,256]{2,1,0:T(8,128)(2,1)} %param.33) | copy-start | bytes 3145732
  176.8 1.2 copy-start.13
  203.9 7.7 %copy-start.10 = (f32[128,2]{0,1:T(2,128)S(1)}, f32[128,2]{0,1:T(2,128)}, u32[]{:S(2)}) copy-start(f32[128,2]{0,1:T(2,128)} %param.32) | copy-start | bytes 3076
  207.0 19.9 %all-to-all-start.1 = ((bf16[8,64,512]{2,1,0:T(8,128)(2,1)}), bf16[8,64,512]{2,1,0:T(8,128)(2,1)S(1)}, u32[]{:S(2)}, u32[]{:S(2)}) async-start(bf16[8,64,512]{2,1,0:T(8,128)(2,1)} %bitcast.55), calls=%async_computation.2 | async-start | bytes 1048576 | tf_op jit(solution)/shard_map/all_to_all | solution.py:150
Sparse Core Ops, SparseCore 0:
  8.9 27.3 all-gather.3
  37.9 25.6 all-gather.5
  81.3 23.1 reduce-scatter.1
  179.5 24.3 all-gather.7
